TPU v7x, 32 devices: a whole 2x2x4 slice. The times are simulated.
32 devices in a mesh: fs: 8 (over z, y), tp: 4 (over x, core).
Axes of the slice: x: 2, y: 2, z: 4, core: 2. Of those that a mesh axis runs over, the one named last changes fastest.
Arguments:
- inputs: bfloat16 [16384, 2048], P('fs'), may hold values from -6 to 6
- attn_out: bfloat16 [16384, 1024], P('fs', 'tp'), may hold values from -6 to 6
- grad_query: bfloat16 [16384, 1024], P('fs', 'tp'), may hold values from -0.125 to 0.125
- grad_key: bfloat16 [16384, 1024], P('fs', 'tp'), may hold values from -0.125 to 0.125
- grad_mixed: bfloat16 [16384, 2048], P('fs'), may hold values from -0.15625 to 0.15625
- query_weight: float32 [2048, 1024], P('fs', 'tp'), may hold values from -0.75 to 0.75
- key_weight: float32 [2048, 1024], P('fs', 'tp'), may hold values from -0.75 to 0.75
- out_weight: float32 [1024, 2048], P('tp', 'fs'), may hold values from -0.75 to 0.75
- factors: bfloat16 [3, 2048, 256], P(None, 'fs'), may hold values from -0.125 to 0.125
- moment_first: float32 [3, 256, 1024], P(None, 'fs', 'tp'), may hold values from -6 to 6
- moment_second: float32 [3, 256, 1024], P(None, 'fs', 'tp'), may hold values from 0.05 to 2
Outputs:
- step_query: float32 [2048, 1024], P('fs', 'tp')
- step_key: float32 [2048, 1024], P('fs', 'tp')
- step_out: float32 [1024, 2048], P('tp', 'fs')
- copy_query: bfloat16 [2048, 1024], P(None, 'tp')
- copy_key: bfloat16 [2048, 1024], P(None, 'tp')
- copy_out: bfloat16 [1024, 2048], P('tp')
- first_new: float32 [3, 256, 1024], P(None, 'fs', 'tp')
- second_new: float32 [3, 256, 1024], P(None, 'fs', 'tp')
All inputs are finite; a program needn't handle non-finite values.
Results may differ from a plain program's by a relative error of at most 0.006.
Values may be sent and summed in bfloat16 or wider, within the bound.
A program may use at most 128 MiB of HBM per device.

v0:
```python
import jax
import jax.numpy as jnp
from jax import lax
from jax.sharding import PartitionSpec as P

RANK = 256
HW = 1024
first_decay = 0.8
second_decay = 0.9
epsilon = 1e-08
learn_rate = 0.02


def over_tokens(left_side, right_side):
    return jnp.dot(left_side.T, right_side, preferred_element_type=jnp.float32)


def moments_update(projected, old_first, old_second):
    first_new = first_decay * old_first + (1.0 - first_decay) * projected
    second_new = second_decay * old_second + (1.0 - second_decay) * projected * projected
    adam_ratio = first_new / (jnp.sqrt(second_new) + epsilon)
    return (first_new, second_new, adam_ratio)


def per_device(
    inputs,
    attn_out,
    grad_query,
    grad_key,
    grad_mixed,
    query_weight,
    key_weight,
    out_weight,
    factors,
    moment_first,
    moment_second,
):
    pairs = ((inputs, grad_query), (inputs, grad_key), (grad_mixed, attn_out))
    partial_value = []
    whole_factors = lax.all_gather(factors, "fs", axis=1, tiled=True)
    for matrix_number in range(3):
        left_side, right_side = pairs[matrix_number]
        mapped = jnp.dot(
            left_side, whole_factors[matrix_number], preferred_element_type=jnp.float32
        )
        upper_part = mapped.astype(jnp.bfloat16)
        lower_part = (mapped - upper_part.astype(jnp.float32)).astype(jnp.bfloat16)
        partial_value.append(
            over_tokens(upper_part, right_side) + over_tokens(lower_part, right_side)
        )
    partial_sums = jnp.stack(partial_value)
    reduced = lax.psum_scatter(partial_sums, "fs", scatter_dimension=1, tiled=True)
    first_new, second_new, adam_ratio = moments_update(reduced, moment_first, moment_second)
    square_total = lax.psum(jnp.sum(adam_ratio * adam_ratio), ("fs", "tp"))
    directions = lax.all_gather(adam_ratio.astype(jnp.bfloat16), "fs", axis=1, tiled=True)
    step_scale = lax.rsqrt(square_total / (3 * RANK * HW) + 1.0)
    step_query = step_scale * jnp.dot(factors[0], directions[0], preferred_element_type=jnp.float32)
    step_key = step_scale * jnp.dot(factors[1], directions[1], preferred_element_type=jnp.float32)
    step_out = step_scale * jnp.dot(factors[2], directions[2], preferred_element_type=jnp.float32).T
    new_query = (query_weight - learn_rate * step_query).astype(jnp.bfloat16)
    new_key = (key_weight - learn_rate * step_key).astype(jnp.bfloat16)
    new_out = (out_weight - learn_rate * step_out).astype(jnp.bfloat16)
    copy_query, copy_key, copy_out = (
        lax.all_gather(new_query, "fs", axis=0, tiled=True),
        lax.all_gather(new_key, "fs", axis=0, tiled=True),
        lax.all_gather(new_out, "fs", axis=1, tiled=True),
    )
    return (step_query, step_key, step_out, copy_query, copy_key, copy_out, first_new, second_new)


def solution(mesh):
    in_specs = (
        P("fs", None),
        P("fs", "tp"),
        P("fs", "tp"),
        P("fs", "tp"),
        P("fs", None),
        P("fs", "tp"),
        P("fs", "tp"),
        P("tp", "fs"),
        P(None, "fs", None),
        P(None, "fs", "tp"),
        P(None, "fs", "tp"),
    )
    out_specs = (
        P("fs", "tp"),
        P("fs", "tp"),
        P("tp", "fs"),
        P(None, "tp"),
        P(None, "tp"),
        P("tp", None),
        P(None, "fs", "tp"),
        P(None, "fs", "tp"),
    )
    return jax.shard_map(
        per_device, mesh=mesh, in_specs=in_specs, out_specs=out_specs, check_vma=False
    )
```

profile of v0, /device:TPU:0, one launch (start us, length us, event | category | flops | bytes accessed | tf_op | source)
XLA Modules:
  0.0 357.2 jit_solution(18089917660759252237)
XLA Ops:
  7.2 0.0 copy-start
  7.2 0.0 all-gather.5.cloned.1.call-start
  7.2 0.7 all-gather.5.cloned.1.call-update
  7.9 0.0 reduce-scatter.2.cloned.1.call-start
  8.0 65.0 %all-gather.5.cloned.1.call-done = bf16[3,2048,256]{2,1,0:T(8,128)(2,1)} async-done(((bf16[3,256,256]{2,1,0:T(8,128)(2,1)}), bf16[3,2048,256]{2,1,0:T(8,128)(2,1)}) %all-gather.5.cloned.1.call-update) | async-done | bytes 3145744 | tf_op jit(solution)/shard_map/all_gather | solution.py:40
  73.0 0.0 copy-start.12
  73.0 6.2 %fusion.6 = f32[2048,256]{1,0:T(8,128)S(1)} fusion(bf16[2048,2048]{1,0:T(8,128)(2,1)} %param.11, bf16[3,2048,256]{2,1,0:T(8,128)(2,1)} %all-gather.5.cloned.1.call-done), kind=kOutput, calls=%fused_computation.17 | convolution fusion | flops 2147483648 | bytes 11534336 | tf_op jit(solution)/shard_map/dot_general | solution.py:43
  79.2 0.0 copy-done
  79.2 0.0 copy-start.13
  79.2 0.5 fusion.12
  79.7 0.0 slice-start
  79.7 0.5 fusion.3
  80.2 0.0 copy-done.12
  80.2 0.9 copy-done.13
  81.1 2.4 fusion.7
  83.6 0.0 copy-done.1
  83.6 0.5 fusion.15
  84.0 0.5 fusion.4
  84.5 0.0 slice-done
  84.5 0.0 slice-done.1
  84.6 0.0 copy-start.2
  84.6 2.4 fusion.5
  87.0 0.0 copy-done.2
  87.0 0.5 fusion.9
  87.5 0.5 fusion.2
  88.0 0.0 copy-start.8
  88.0 0.0 copy-start.10
  88.0 0.0 copy-start.11
  88.0 0.0 copy-start.3
  88.1 0.9 pad_maximum_fusion
  89.0 0.0 reduce-scatter.2.cloned.1.call-update
  89.0 0.0 copy-start.9
  89.0 0.0 all-gather.11.cloned.1.call-start
  89.1 0.0 copy-done.8
  89.1 0.1 copy.24
  89.2 62.6 %reduce-scatter.2.cloned.1.call-done = f32[3,32,256]{2,1,0:T(8,128)} async-done(((f32[3,256,256]{2,1,0:T(8,128)}), f32[3,32,256]{2,1,0:T(8,128)}) %reduce-scatter.2.cloned.1.call-update) | async-done | bytes 98320 | tf_op jit(solution)/shard_map/reduce_scatter | solution.py:52
  151.8 0.0 copy-done.10
  151.8 0.0 copy-done.11
  151.8 1.6 multiply_reduce_fusion
  153.4 31.2 %all_gather.16 = bf16[3,256,256]{2,1,0:T(8,128)(2,1)S(1)} all-gather(bf16[3,32,256]{2,1,0:T(8,128)(2,1)S(1)} %fusion.24), channel_id=1, replica_groups=mesh['fs'=8,'tp'=4] {'fs'}, dimensions={1}, use_global_device_ids=true | all-gather | bytes 442368 | tf_op jit(solution)/shard_map/all_gather | solution.py:55
  184.6 37.6 %psum.7 = f32[]{:T(128)} all-reduce(f32[]{:T(128)} %get-tuple-element.16), channel_id=1, replica_groups=mesh['fs'=8,'tp'=4] {'fs','tp'}, use_global_device_ids=true, to_apply=%region_2.0 | all-reduce | flops 1 | bytes 8 | tf_op jit(solution)/shard_map/psum | solution.py:54
  222.9 0.0 copy-done.3
  222.9 0.8 subtract_convert_fusion.6
  223.8 0.0 all-gather.11.cloned.1.call-update
  223.8 0.0 all-gather.9.cloned.1.call-start
  223.8 0.0 copy-done.7
  223.8 0.9 subtract_convert_fusion.7
  224.8 0.0 all-gather.9.cloned.1.call-update
  224.8 0.0 all-gather.7.cloned.1.call-start
  224.9 0.0 copy-done.9
  224.9 0.1 copy.22
  225.0 0.9 subtract_convert_fusion.8
  225.9 0.0 copy-done.5
  225.9 0.0 copy-done.6
  225.9 0.0 all-gather.7.cloned.1.call-update
  225.9 0.8 copy.26
  226.8 0.8 copy.25
  227.6 37.6 %all-gather.11.cloned.1.call-done = bf16[256,2048]{0,1:T(8,128)(2,1)} async-done(((bf16[256,256]{0,1:T(8,128)(2,1)}), bf16[256,2048]{0,1:T(8,128)(2,1)}) %all-gather.11.cloned.1.call-update) | async-done | bytes 1048592 | tf_op jit(solution)/shard_map/all_gather | solution.py:66
  265.2 2.3 copy.28
  267.5 39.3 %all-gather.9.cloned.1.call-done = bf16[2048,256]{1,0:T(8,128)(2,1)} async-done(((bf16[256,256]{1,0:T(8,128)(2,1)}), bf16[2048,256]{1,0:T(8,128)(2,1)}) %all-gather.9.cloned.1.call-update) | async-done | bytes 1048592 | tf_op jit(solution)/shard_map/all_gather | solution.py:65
  306.8 40.6 %all-gather.7.cloned.1.call-done = bf16[2048,256]{0,1:T(8,128)(2,1)} async-done(((bf16[256,256]{0,1:T(8,128)(2,1)}), bf16[2048,256]{0,1:T(8,128)(2,1)}) %all-gather.7.cloned.1.call-update) | async-done | bytes 1048592 | tf_op jit(solution)/shard_map/all_gather | solution.py:64
  347.4 2.3 copy.27
  349.7 0.0 copy-done.4
  349.7 1.0 copy.32
  (8 shorter events, 0.1 us)
Async XLA Ops:
  7.2 72.0 %copy-start = (bf16[2048,256]{1,0:T(8,128)(2,1)S(1)}, bf16[2048,256]{1,0:T(8,128)(2,1)}, u32[]{:S(2)}) copy-start(bf16[2048,256]{1,0:T(8,128)(2,1)} %param.14) | copy-start | bytes 3145732
  7.2 65.8 %all-gather.5.cloned.1.call-start = ((), (), s32[]{:S(2)}) async-start(), calls=%async_computation.1 | async-start | bytes 3538944 | tf_op jit(solution)/shard_map/all_gather | solution.py:40
  7.9 143.9 %reduce-scatter.2.cloned.1.call-start = ((), (), s32[]{:S(2)}) async-start(), calls=%async_computation.2 | async-start | bytes 884736 | tf_op jit(solution)/shard_map/reduce_scatter | solution.py:52
  73.0 7.3 %copy-start.12 = (bf16[2048,2048]{1,0:T(8,128)(2,1)S(1)}, bf16[2048,2048]{1,0:T(8,128)(2,1)}, u32[]{:S(2)}) copy-start(bf16[2048,2048]{1,0:T(8,128)(2,1)} %param.11) | copy-start | bytes 25165828
  79.2 1.9 copy-start.13
  79.7 4.8 %slice-start = ((s8[8388608]{0:T(1024)(128)(4,1)}), s8[4194304]{0:T(1024)(128)(4,1)S(1)}, s32[]{:S(2)}) async-start(s8[8388608]{0:T(1024)(128)(4,1)} %bitcast.58), calls=%async_computation.6 | async-start | bytes 8388608
  81.1 2.5 copy-start.1
  81.1 3.4 slice-start.1
  84.6 2.5 copy-start.2
  88.0 1.1 copy-start.8
  88.0 63.8 %copy-start.10 = (f32[3,32,256]{2,1,0:T(8,128)S(1)}, f32[3,32,256]{2,1,0:T(8,128)}, u32[]{:S(2)}) copy-start(f32[3,32,256]{2,1,0:T(8,128)} %param.21) | copy-start | bytes 294916
  88.0 63.8 %copy-start.11 = (f32[3,32,256]{2,1,0:T(8,128)S(1)}, f32[3,32,256]{2,1,0:T(8,128)}, u32[]{:S(2)}) copy-start(f32[3,32,256]{2,1,0:T(8,128)} %param.20) | copy-start | bytes 294916
  88.0 134.9 %copy-start.3 = (bf16[3,256,256]{2,1,0:T(8,128)(2,1)S(1)}, bf16[3,256,256]{2,1,0:T(8,128)(2,1)}, u32[]{:S(2)}) copy-start(bf16[3,256,256]{2,1,0:T(8,128)(2,1)} %param.19) | copy-start | bytes 1179652
  89.0 134.9 %copy-start.7 = (f32[256,256]{1,0:T(8,128)S(1)}, f32[256,256]{1,0:T(8,128)}, u32[]{:S(2)}) copy-start(f32[256,256]{1,0:T(8,128)} %param.17) | copy-start | bytes 786436
  89.0 135.8 %copy-start.9 = (f32[256,256]{1,0:T(8,128)S(1)}, f32[256,256]{1,0:T(8,128)}, u32[]{:S(2)}) copy-start(f32[256,256]{1,0:T(8,128)} %param.16) | copy-start | bytes 786436
  89.0 176.2 %all-gather.11.cloned.1.call-start = ((), (), s32[]{:S(2)}) async-start(), calls=%async_computation.5 | async-start | bytes 1179648 | tf_op jit(solution)/shard_map/all_gather | solution.py:66
  153.4 72.5 %copy-start.5 = (f32[3,32,256]{2,1,0:T(8,128)}, f32[3,32,256]{2,1,0:T(8,128)S(1)}, u32[]{:S(2)}) copy-start(f32[3,32,256]{2,1,0:T(8,128)S(1)} %get-tuple-element.40) | copy-start | bytes 294916
  153.4 72.5 %copy-start.6 = (f32[3,32,256]{2,1,0:T(8,128)}, f32[3,32,256]{2,1,0:T(8,128)S(1)}, u32[]{:S(2)}) copy-start(f32[3,32,256]{2,1,0:T(8,128)S(1)} %get-tuple-element.39) | copy-start | bytes 294916
  223.8 83.0 %all-gather.9.cloned.1.call-start = ((), (), s32[]{:S(2)}) async-start(), calls=%async_computation.4 | async-start | bytes 1179648 | tf_op jit(solution)/shard_map/all_gather | solution.py:65
  224.8 122.6 %all-gather.7.cloned.1.call-start = ((), (), s32[]{:S(2)}) async-start(), calls=%async_computation.3 | async-start | bytes 1179648 | tf_op jit(solution)/shard_map/all_gather | solution.py:64
  306.8 42.9 %copy-start.4 = (bf16[2048,256]{1,0:T(8,128)(2,1)S(1)}, bf16[2048,256]{1,0:T(8,128)(2,1)}, u32[]{:S(2)}) copy-start(bf16[2048,256]{1,0:T(8,128)(2,1)} %all-gather.9.cloned.1.call-done) | copy-start | bytes 3145732
Sparse Core Ops, SparseCore 0:
  10.2 62.7 all-gather.4
  89.1 62.6 reduce-scatter.1
  223.9 41.2 all-gather.10
  267.8 38.9 all-gather.8
  309.3 38.0 all-gather.6
where the time goes:
time: 358 us; the launch traced here: 357 us
  waiting for transfers between devices  246 us (69%)
  blocking collectives  68.8 us (19%)
  matrix products  16.7 us (5%)
  between operations  14.7 us (4%)
  local copies, waits for them, and re-layouts  8.36 us (2%)
    all_gather x1, waiting for transfers between devices, per_device(): whole_factors = lax.all_gather(factors, 'fs', axis=1, tiled=True)  65 us
    reduce_scatter x1, waiting for transfers between devices, per_device(): lax.psum_scatter(partial_sums, 'fs', scatter_dimension=1, tiled=True)  62.6 us
    all_gather x1, waiting for transfers between devices, per_device(): lax.all_gather(new_query, 'fs', axis=0, tiled=True)  40.6 us
    all_gather x1, waiting for transfers between devices, per_device(): lax.all_gather(new_key, 'fs', axis=0, tiled=True)  39.3 us
    all_gather x1, waiting for transfers between devices, per_device(): lax.all_gather(new_out, 'fs', axis=1, tiled=True)  37.6 us
    psum x1, blocking collectives, per_device(): square_total = lax.psum(jnp.sum(adam_ratio * adam_ratio), ('fs', 'tp'))  37.6 us
    all_gather x1, blocking collectives, per_device(): lax.all_gather(adam_ratio.astype(jnp.bfloat16), 'fs', axis=1, tiled=True)  31.2 us
    dot_general x3, matrix products, per_device(): jnp.dot(left_side, whole_factors[matrix_number], preferred_element_type=j...  11.1 us
  transfers between devices with their start and end apart: 5, of which 5 were waited for; matrix products, arithmetic and copies ran while one was open for 2% of the time, Pallas kernels for 0%

commit v1 on v0

--- a/solution.py
+++ b/solution.py
@@ -9,6 +9,7 @@
 second_decay = 0.9
 epsilon = 1e-08
 learn_rate = 0.02
+switch_rails = lambda sample: jnp.concatenate(lax.all_gather(sample, "fs"), axis=1)
 
 
 def over_tokens(left_side, right_side):
@@ -52,7 +53,7 @@
     reduced = lax.psum_scatter(partial_sums, "fs", scatter_dimension=1, tiled=True)
     first_new, second_new, adam_ratio = moments_update(reduced, moment_first, moment_second)
     square_total = lax.psum(jnp.sum(adam_ratio * adam_ratio), ("fs", "tp"))
-    directions = lax.all_gather(adam_ratio.astype(jnp.bfloat16), "fs", axis=1, tiled=True)
+    directions = switch_rails(adam_ratio.astype(jnp.bfloat16))
     step_scale = lax.rsqrt(square_total / (3 * RANK * HW) + 1.0)
     step_query = step_scale * jnp.dot(factors[0], directions[0], preferred_element_type=jnp.float32)
     step_key = step_scale * jnp.dot(factors[1], directions[1], preferred_element_type=jnp.float32)

time: 358 us -> 358 us (level)
  no operation moved by 1% of the time
where the time goes in v1:
time: 358 us; the launch traced here: 357 us
  waiting for transfers between devices  246 us (69%)
  blocking collectives  68.8 us (19%)
  matrix products  16.7 us (5%)
  between operations  14.7 us (4%)
  local copies, waits for them, and re-layouts  8.39 us (2%)
    all_gather x1, waiting for transfers between devices, per_device(): whole_factors = lax.all_gather(factors, 'fs', axis=1, tiled=True)  65 us
    reduce_scatter x1, waiting for transfers between devices, per_device(): lax.psum_scatter(partial_sums, 'fs', scatter_dimension=1, tiled=True)  62.6 us
    all_gather x1, waiting for transfers between devices, per_device(): lax.all_gather(new_query, 'fs', axis=0, tiled=True)  40.6 us
    all_gather x1, waiting for transfers between devices, per_device(): lax.all_gather(new_key, 'fs', axis=0, tiled=True)  39.3 us
    psum x1, blocking collectives, per_device(): square_total = lax.psum(jnp.sum(adam_ratio * adam_ratio), ('fs', 'tp'))  37.7 us
    all_gather x1, waiting for transfers between devices, per_device(): lax.all_gather(new_out, 'fs', axis=1, tiled=True)  37.6 us
    all_gather x1, blocking collectives, lax.all_gather(sample, 'fs')  31.2 us
    dot_general x3, matrix products, per_device(): jnp.dot(left_side, whole_factors[matrix_number], preferred_element_type=j...  11.1 us
  transfers between devices with their start and end apart: 5, of which 5 were waited for; matrix products, arithmetic and copies ran while one was open for 2% of the time, Pallas kernels for 0%

profile of v1, /device:TPU:0, one launch (start us, length us, event | category | flops | bytes accessed | tf_op | source)
XLA Modules:
  0.0 357.3 jit_solution(6425890490261995462)
XLA Ops:
  7.2 0.0 copy-start
  7.2 0.0 all-gather.6.cloned.1.call-start
  7.2 0.7 all-gather.6.cloned.1.call-update
  7.9 0.0 reduce-scatter.2.cloned.1.call-start
  8.0 65.0 %all-gather.6.cloned.1.call-done = bf16[3,2048,256]{2,1,0:T(8,128)(2,1)} async-done(((bf16[3,256,256]{2,1,0:T(8,128)(2,1)}), bf16[3,2048,256]{2,1,0:T(8,128)(2,1)}) %all-gather.6.cloned.1.call-update) | async-done | bytes 3145744 | tf_op jit(solution)/shard_map/all_gather | solution.py:41
  73.0 0.0 copy-start.12
  73.0 6.2 %fusion.6 = f32[2048,256]{1,0:T(8,128)S(1)} fusion(bf16[2048,2048]{1,0:T(8,128)(2,1)} %param.11, bf16[3,2048,256]{2,1,0:T(8,128)(2,1)} %all-gather.6.cloned.1.call-done), kind=kOutput, calls=%fused_computation.17 | convolution fusion | flops 2147483648 | bytes 11534336 | tf_op jit(solution)/shard_map/dot_general | solution.py:44
  79.2 0.0 copy-done
  79.2 0.0 copy-start.13
  79.2 0.5 fusion.12
  79.7 0.0 slice-start
  79.7 0.5 fusion.3
  80.2 0.0 copy-done.12
  80.2 0.9 copy-done.13
  81.1 2.4 fusion.7
  83.6 0.0 copy-done.1
  83.6 0.5 fusion.15
  84.0 0.5 fusion.4
  84.5 0.0 slice-done
  84.5 0.0 slice-done.1
  84.6 0.0 copy-start.2
  84.6 2.4 fusion.5
  87.0 0.0 copy-done.2
  87.0 0.5 fusion.9
  87.5 0.5 fusion.2
  88.0 0.0 copy-start.8
  88.0 0.0 copy-start.10
  88.0 0.0 copy-start.11
  88.0 0.0 copy-start.3
  88.1 0.9 pad_maximum_fusion
  89.0 0.0 reduce-scatter.2.cloned.1.call-update
  89.0 0.0 all-gather.12.cloned.1.call-start
  89.1 0.0 copy-done.8
  89.1 0.1 copy.34
  89.2 0.0 copy-start.9
  89.2 62.6 %reduce-scatter.2.cloned.1.call-done = f32[3,32,256]{2,1,0:T(8,128)} async-done(((f32[3,256,256]{2,1,0:T(8,128)}), f32[3,32,256]{2,1,0:T(8,128)}) %reduce-scatter.2.cloned.1.call-update) | async-done | bytes 98320 | tf_op jit(solution)/shard_map/reduce_scatter | solution.py:53
  151.8 0.0 copy-done.10
  151.8 0.0 copy-done.11
  151.8 1.6 multiply_reduce_fusion
  153.4 31.2 %all-gather = bf16[24,32,256]{2,1,0:T(8,128)(2,1)S(1)} all-gather(bf16[3,32,256]{2,1,0:T(8,128)(2,1)S(1)} %fusion.24), channel_id=2, replica_groups=mesh['fs'=8,'tp'=4] {'fs'}, dimensions={0}, use_global_device_ids=true | all-gather | bytes 442368 | tf_op jit(solution)/shard_map/all_gather | solution.py:12
  184.7 37.7 %psum.7 = f32[]{:T(128)} all-reduce(f32[]{:T(128)} %get-tuple-element.24), channel_id=1, replica_groups=mesh['fs'=8,'tp'=4] {'fs','tp'}, use_global_device_ids=true, to_apply=%region_2.0 | all-reduce | flops 1 | bytes 8 | tf_op jit(solution)/shard_map/psum | solution.py:55
  223.0 0.0 copy-done.3
  223.0 0.9 subtract_convert_fusion.6
  223.9 0.0 all-gather.12.cloned.1.call-update
  223.9 0.0 all-gather.10.cloned.1.call-start
  223.9 0.0 copy-done.7
  223.9 0.9 subtract_convert_fusion.7
  224.9 0.0 all-gather.10.cloned.1.call-update
  224.9 0.0 all-gather.8.cloned.1.call-start
  225.0 0.0 copy-done.9
  225.0 0.1 copy.32
  225.1 0.9 subtract_convert_fusion.8
  226.0 0.0 copy-done.5
  226.0 0.0 copy-done.6
  226.0 0.0 all-gather.8.cloned.1.call-update
  226.0 0.8 copy.36
  226.9 0.8 copy.35
  227.7 37.6 %all-gather.12.cloned.1.call-done = bf16[256,2048]{0,1:T(8,128)(2,1)} async-done(((bf16[256,256]{0,1:T(8,128)(2,1)}), bf16[256,2048]{0,1:T(8,128)(2,1)}) %all-gather.12.cloned.1.call-update) | async-done | bytes 1048592 | tf_op jit(solution)/shard_map/all_gather | solution.py:67
  265.3 2.3 copy.38
  267.6 39.3 %all-gather.10.cloned.1.call-done = bf16[2048,256]{1,0:T(8,128)(2,1)} async-done(((bf16[256,256]{1,0:T(8,128)(2,1)}), bf16[2048,256]{1,0:T(8,128)(2,1)}) %all-gather.10.cloned.1.call-update) | async-done | bytes 1048592 | tf_op jit(solution)/shard_map/all_gather | solution.py:66
  306.9 40.6 %all-gather.8.cloned.1.call-done = bf16[2048,256]{0,1:T(8,128)(2,1)} async-done(((bf16[256,256]{0,1:T(8,128)(2,1)}), bf16[2048,256]{0,1:T(8,128)(2,1)}) %all-gather.8.cloned.1.call-update) | async-done | bytes 1048592 | tf_op jit(solution)/shard_map/all_gather | solution.py:65
  347.5 2.3 copy.37
  349.8 0.0 copy-done.4
  349.8 1.0 copy.42
  (9 shorter events, 0.1 us)
Async XLA Ops:
  7.2 72.0 %copy-start = (bf16[2048,256]{1,0:T(8,128)(2,1)S(1)}, bf16[2048,256]{1,0:T(8,128)(2,1)}, u32[]{:S(2)}) copy-start(bf16[2048,256]{1,0:T(8,128)(2,1)} %param.14) | copy-start | bytes 3145732
  7.2 65.8 %all-gather.6.cloned.1.call-start = ((), (), s32[]{:S(2)}) async-start(), calls=%async_computation.1 | async-start | bytes 3538944 | tf_op jit(solution)/shard_map/all_gather | solution.py:41
  7.9 143.9 %reduce-scatter.2.cloned.1.call-start = ((), (), s32[]{:S(2)}) async-start(), calls=%async_computation.2 | async-start | bytes 884736 | tf_op jit(solution)/shard_map/reduce_scatter | solution.py:53
  73.0 7.3 %copy-start.12 = (bf16[2048,2048]{1,0:T(8,128)(2,1)S(1)}, bf16[2048,2048]{1,0:T(8,128)(2,1)}, u32[]{:S(2)}) copy-start(bf16[2048,2048]{1,0:T(8,128)(2,1)} %param.11) | copy-start | bytes 25165828
  79.2 1.9 copy-start.13
  79.7 4.8 %slice-start = ((s8[8388608]{0:T(1024)(128)(4,1)}), s8[4194304]{0:T(1024)(128)(4,1)S(1)}, s32[]{:S(2)}) async-start(s8[8388608]{0:T(1024)(128)(4,1)} %bitcast.56), calls=%async_computation.6 | async-start | bytes 8388608
  81.1 2.5 copy-start.1
  81.1 3.4 slice-start.1
  84.6 2.5 copy-start.2
  88.0 1.1 copy-start.8
  88.0 63.8 %copy-start.10 = (f32[3,32,256]{2,1,0:T(8,128)S(1)}, f32[3,32,256]{2,1,0:T(8,128)}, u32[]{:S(2)}) copy-start(f32[3,32,256]{2,1,0:T(8,128)} %param.21) | copy-start | bytes 294916
  88.0 63.8 %copy-start.11 = (f32[3,32,256]{2,1,0:T(8,128)S(1)}, f32[3,32,256]{2,1,0:T(8,128)}, u32[]{:S(2)}) copy-start(f32[3,32,256]{2,1,0:T(8,128)} %param.20) | copy-start | bytes 294916
  88.0 135.0 %copy-start.3 = (bf16[3,256,256]{2,1,0:T(8,128)(2,1)S(1)}, bf16[3,256,256]{2,1,0:T(8,128)(2,1)}, u32[]{:S(2)}) copy-start(bf16[3,256,256]{2,1,0:T(8,128)(2,1)} %param.19) | copy-start | bytes 1179652
  89.0 135.0 %copy-start.7 = (f32[256,256]{1,0:T(8,128)S(1)}, f32[256,256]{1,0:T(8,128)}, u32[]{:S(2)}) copy-start(f32[256,256]{1,0:T(8,128)} %param.17) | copy-start | bytes 786436
  89.0 176.3 %all-gather.12.cloned.1.call-start = ((), (), s32[]{:S(2)}) async-start(), calls=%async_computation.5 | async-start | bytes 1179648 | tf_op jit(solution)/shard_map/all_gather | solution.py:67
  89.2 135.8 %copy-start.9 = (f32[256,256]{1,0:T(8,128)S(1)}, f32[256,256]{1,0:T(8,128)}, u32[]{:S(2)}) copy-start(f32[256,256]{1,0:T(8,128)} %param.16) | copy-start | bytes 786436
  153.4 72.6 %copy-start.5 = (f32[3,32,256]{2,1,0:T(8,128)}, f32[3,32,256]{2,1,0:T(8,128)S(1)}, u32[]{:S(2)}) copy-start(f32[3,32,256]{2,1,0:T(8,128)S(1)} %get-tuple-element.51) | copy-start | bytes 294916
  153.4 72.6 %copy-start.6 = (f32[3,32,256]{2,1,0:T(8,128)}, f32[3,32,256]{2,1,0:T(8,128)S(1)}, u32[]{:S(2)}) copy-start(f32[3,32,256]{2,1,0:T(8,128)S(1)} %get-tuple-element.50) | copy-start | bytes 294916
  223.9 83.0 %all-gather.10.cloned.1.call-start = ((), (), s32[]{:S(2)}) async-start(), calls=%async_computation.4 | async-start | bytes 1179648 | tf_op jit(solution)/shard_map/all_gather | solution.py:66
  224.9 122.6 %all-gather.8.cloned.1.call-start = ((), (), s32[]{:S(2)}) async-start(), calls=%async_computation.3 | async-start | bytes 1179648 | tf_op jit(solution)/shard_map/all_gather | solution.py:65
  306.9 42.9 %copy-start.4 = (bf16[2048,256]{1,0:T(8,128)(2,1)S(1)}, bf16[2048,256]{1,0:T(8,128)(2,1)}, u32[]{:S(2)}) copy-start(bf16[2048,256]{1,0:T(8,128)(2,1)} %all-gather.10.cloned.1.call-done) | copy-start | bytes 3145732
Sparse Core Ops, SparseCore 0:
  10.2 62.7 all-gather.5
  89.1 62.6 reduce-scatter.1
  224.0 41.2 all-gather.11
  267.9 38.9 all-gather.9
  309.4 38.0 all-gather.7
